TPU v7x, 32 devices: a whole 2x2x4 slice. The times are simulated.
32 devices in a mesh: fs: 8 (over z, y), tp: 4 (over x, core).
Axes of the slice: x: 2, y: 2, z: 4, core: 2. Of those that a mesh axis runs over, the one named last changes fastest.
Arguments:
- tokens: bfloat16 [4096, 2048], P(('fs', 'tp')), may hold values from -6 to 6
- gate_proj: bfloat16 [2048, 512], P('fs', 'tp'), may hold values from -0.125 to 0.125
- signal_proj: bfloat16 [2048, 512], P('fs', 'tp'), may hold values from -1.5467961 to 1.5467961
- spatial: bfloat16 [4, 128, 128], replicated, may hold values from -0.5 to 0.5
- signal_gain: bfloat16 [512], P('tp'), may hold values from 0.099609375 to 1.8984375
- mixer_out: bfloat16 [512, 2048], P('tp', 'fs'), may hold values from -0.25 to 0.25
- mixer_gain: bfloat16 [2048], replicated, may hold values from 0.099609375 to 1.8984375
- ffn_gate: bfloat16 [2048, 5632], P('fs', 'tp'), may hold values from -0.125 to 0.125
- ffn_value: bfloat16 [2048, 5632], P('fs', 'tp'), may hold values from -0.125 to 0.125
- conv_taps: bfloat16 [3, 5632], P(None, 'tp'), may hold values from -3.5 to 3.5
- ffn_down: bfloat16 [5632, 2048], P('tp', 'fs'), may hold values from -0.078125 to 0.078125
- output_gain: bfloat16 [2048], replicated, may hold values from 0.099609375 to 1.8984375
Outputs:
- result: bfloat16 [4096, 2048], P(('fs', 'tp'))
All inputs are finite; a program needn't handle non-finite values.
Results may differ from a plain program's by a relative error of at most 0.01.
Values may be sent and summed in bfloat16 or wider, within the bound.
A program may use at most 64 MiB of HBM per device.

v0:
```python
import math

import jax
import jax.numpy as jnp
from jax import lax
from jax.sharding import PartitionSpec as P

MIX_WIDTH = 512
HEAD_SIZE = 128
BLOCK = 128
SEGMENT = 64


EPSILON = 1e-05
RESIDUAL_SCALE = math.sqrt(2.0)


def normalize(values):
    row_mean = jnp.mean(values, axis=-1, keepdims=True)
    centred = values - row_mean
    spread = jnp.mean(centred * centred, axis=-1, keepdims=True)
    return centred * lax.rsqrt(spread + EPSILON)


def causal_conv(gate_pre, conv_taps):
    taps = conv_taps.astype(jnp.float32)
    width = gate_pre.shape[1]
    shifted_one = jnp.concatenate([jnp.zeros((1, width), jnp.float32), gate_pre[:-1]], axis=0)
    shifted_two = jnp.concatenate([jnp.zeros((2, width), jnp.float32), gate_pre[:-2]], axis=0)
    return taps[0] * shifted_two + taps[1] * shifted_one + taps[2] * gate_pre


def shards(
    tokens,
    gate_proj,
    signal_proj,
    spatial,
    signal_gain,
    mixer_out,
    mixer_gain,
    ffn_gate,
    ffn_value,
    conv_taps,
    ffn_down,
    output_gain,
):
    residual = tokens.astype(jnp.float32)
    mix_input = normalize(residual).astype(jnp.bfloat16)
    segment_ids = jnp.arange(BLOCK) // SEGMENT
    allowed = segment_ids[None, :] <= segment_ids[:, None]
    masked = jnp.where(allowed[None], spatial, jnp.zeros_like(spatial))
    group_input = lax.all_gather(mix_input, "tp", axis=0, tiled=True)
    group_rows = group_input.shape[0]
    column_count = gate_proj.shape[1]
    pieces = (
        lax.all_gather(gate_proj, "fs", axis=0, tiled=True),
        lax.all_gather(signal_proj, "fs", axis=0, tiled=True),
    )
    left_part = group_input
    gate_sum = jnp.dot(left_part, pieces[0], preferred_element_type=jnp.float32)
    signal_sum = jnp.dot(left_part, pieces[1], preferred_element_type=jnp.float32)
    branch_gate = jax.nn.gelu(gate_sum)
    branch_signal = jax.nn.gelu(signal_sum)
    total_sum, square_sum = lax.psum(
        (jnp.sum(branch_signal, axis=1), jnp.sum(branch_signal * branch_signal, axis=1)), "tp"
    )
    row_mean = total_sum / MIX_WIDTH
    spread = square_sum / MIX_WIDTH - row_mean * row_mean
    spatial_input = (
        (branch_signal - row_mean[:, None])
        * lax.rsqrt(spread[:, None] + EPSILON)
        * signal_gain.astype(jnp.float32)
    ).astype(jnp.bfloat16)
    head_index = lax.axis_index("tp") * column_count // HEAD_SIZE
    own_weights = lax.dynamic_index_in_dim(masked, head_index, 0, keepdims=False)
    blocks = spatial_input.reshape(group_rows // BLOCK, BLOCK, column_count)
    mixed_rows = jnp.einsum(
        "ij,njc->nic", own_weights, blocks, preferred_element_type=jnp.float32
    ).reshape(group_rows, column_count)
    gated_rows = (branch_gate * mixed_rows).astype(jnp.bfloat16)
    out_columns = lax.all_gather(mixer_out, "fs", axis=1, tiled=True)
    selected = gated_rows
    mix_out = lax.psum_scatter(
        jnp.dot(selected, out_columns, preferred_element_type=jnp.float32).astype(jnp.bfloat16),
        "tp",
        scatter_dimension=0,
        tiled=True,
    ).astype(jnp.float32)
    middle = (
        normalize(RESIDUAL_SCALE * residual + mix_out) * mixer_gain.astype(jnp.float32)
    ).astype(jnp.bfloat16)
    middle_wide = middle.astype(jnp.float32)
    ffn_input = normalize(middle_wide).astype(jnp.bfloat16)
    group_ffn = lax.all_gather(ffn_input, "tp", axis=0, tiled=True)
    pieces = (
        lax.all_gather(ffn_gate, "fs", axis=0, tiled=True),
        lax.all_gather(ffn_value, "fs", axis=0, tiled=True),
    )
    left_part = group_ffn
    gate_pre = jnp.dot(left_part, pieces[0], preferred_element_type=jnp.float32)
    value_pre = jnp.dot(left_part, pieces[1], preferred_element_type=jnp.float32)
    whole_down = lax.all_gather(ffn_down, "fs", axis=1, tiled=True)
    hidden = (jax.nn.silu(causal_conv(gate_pre, conv_taps)) * value_pre).astype(jnp.bfloat16)
    selected = hidden
    ffn_out = lax.psum_scatter(
        jnp.dot(selected, whole_down, preferred_element_type=jnp.float32).astype(jnp.bfloat16),
        "tp",
        scatter_dimension=0,
        tiled=True,
    ).astype(jnp.float32)
    return (
        normalize(RESIDUAL_SCALE * middle_wide + ffn_out) * output_gain.astype(jnp.float32)
    ).astype(jnp.bfloat16)


def solution(mesh):
    in_specs = (
        P(("fs", "tp"), None),
        P("fs", "tp"),
        P("fs", "tp"),
        P(),
        P("tp"),
        P("tp", "fs"),
        P(),
        P("fs", "tp"),
        P("fs", "tp"),
        P(None, "tp"),
        P("tp", "fs"),
        P(),
    )
    out_specs = P(("fs", "tp"), None)
    return jax.shard_map(shards, mesh=mesh, in_specs=in_specs, out_specs=out_specs, check_vma=False)
```

profile of v0, /device:TPU:0, one launch (start us, length us, event | category | flops | bytes accessed | tf_op | source)
XLA Modules:
  0.0 485.2 jit_solution(16382907867453121920)
XLA Ops:
  7.4 1.2 convert_reduce_fusion.1
  8.6 1.3 fusion.7
  9.9 2.2 fusion.8
  12.2 0.7 convert_element_type.53
  13.0 33.3 %all_gather.26 = bf16[2048,128]{1,0:T(8,128)(2,1)S(1)} all-gather(bf16[256,128]{1,0:T(8,128)(2,1)} %param.14), channel_id=1, replica_groups=mesh['fs'=8,'tp'=4] {'fs'}, dimensions={0}, use_global_device_ids=true | all-gather | bytes 589824 | tf_op jit(solution)/shard_map/all_gather | solution.py:57
  46.3 31.5 %all_gather.25 = bf16[2048,128]{1,0:T(8,128)(2,1)S(1)} all-gather(bf16[256,128]{1,0:T(8,128)(2,1)S(1)} %copy-done.1), channel_id=1, replica_groups=mesh['fs'=8,'tp'=4] {'fs'}, dimensions={0}, use_global_device_ids=true | all-gather | bytes 589824 | tf_op jit(solution)/shard_map/all_gather | solution.py:56
  77.8 31.2 %all_gather.27 = bf16[128,2048]{1,0:T(8,128)(2,1)S(1)} all-gather(bf16[128,256]{1,0:T(8,128)(2,1)S(1)} %copy-done.2), channel_id=1, replica_groups=mesh['fs'=8,'tp'=4] {'fs'}, dimensions={1}, use_global_device_ids=true | all-gather | bytes 589824 | tf_op jit(solution)/shard_map/all_gather | solution.py:81
  109.0 2.4 fusion.38
  111.4 5.7 %all-reduce.2 = (f32[512]{0:T(512)S(1)}, f32[512]{0:T(512)S(1)}) all-reduce(f32[512]{0:T(512)S(1)} %get-tuple-element.6, f32[512]{0:T(512)S(1)} %get-tuple-element.5), channel_id=1, replica_groups=mesh['fs'=8,'tp'=4] {'tp'}, use_global_device_ids=true, to_apply=%region_5.6 | all-reduce | flops 1024 | bytes 8192 | tf_op jit(solution)/shard_map/psum | solution.py:64
  117.3 0.9 fusion.30
  118.2 2.3 fusion.21
  120.6 2.0 convolution_convert_fusion
  122.7 0.5 all-gather.10.cloned.1.call-update
  123.3 31.8 %reduce-scatter.3.cloned.1.call-done = bf16[128,2048]{1,0:T(8,128)(2,1)} async-done(((bf16[512,2048]{1,0:T(8,128)(2,1)}), bf16[128,2048]{1,0:T(8,128)(2,1)}) %reduce-scatter.3.cloned.1.call-update) | async-done | bytes 524304 | tf_op jit(solution)/shard_map/reduce_scatter | solution.py:83
  155.1 1.3 fusion.12
  156.4 1.4 multiply_reduce_fusion.1
  157.8 1.4 convert_reduce_fusion
  159.3 0.3 fusion.5
  159.6 1.1 fusion.6
  160.7 0.5 all-gather.12.cloned.1.call-update
  161.3 0.7 all-gather.14.cloned.1.call-update
  162.0 0.2 reduce-scatter.5.cloned.1.call-start
  162.3 56.3 %all-gather.10.cloned.1.call-done = bf16[2048,1408]{1,0:T(8,128)(2,1)} async-done(((bf16[256,1408]{1,0:T(8,128)(2,1)}), bf16[2048,1408]{1,0:T(8,128)(2,1)}) %all-gather.10.cloned.1.call-update) | async-done | bytes 5767184 | tf_op jit(solution)/shard_map/all_gather | solution.py:96
  218.6 22.0 %all-gather.8.cloned.1.call-done = bf16[512,2048]{1,0:T(8,128)(2,1)} async-done(((bf16[128,2048]{1,0:T(8,128)(2,1)}), bf16[512,2048]{1,0:T(8,128)(2,1)}) %all-gather.8.cloned.1.call-update) | async-done | bytes 2097168 | tf_op jit(solution)/shard_map/all_gather | solution.py:94
  240.6 8.4 %fusion.39 = f32[512,1408]{1,0:T(8,128)} fusion(bf16[512,2048]{1,0:T(8,128)(2,1)} %all-gather.8.cloned.1.call-done, bf16[2048,1408]{1,0:T(8,128)(2,1)} %all-gather.10.cloned.1.call-done), kind=kOutput, calls=%fused_computation.74 | convolution fusion | flops 2952790016 | bytes 10747904 | tf_op jit(solution)/shard_map/dot_general | solution.py:100
  249.0 85.8 %all-gather.12.cloned.1.call-done = bf16[2048,1408]{1,0:T(8,128)(2,1)} async-done(((bf16[256,1408]{1,0:T(8,128)(2,1)}), bf16[2048,1408]{1,0:T(8,128)(2,1)}) %all-gather.12.cloned.1.call-update) | async-done | bytes 5767184 | tf_op jit(solution)/shard_map/all_gather | solution.py:97
  334.8 93.1 %all-gather.14.cloned.1.call-done = bf16[1408,2048]{1,0:T(8,128)(2,1)} async-done(((bf16[1408,256]{1,0:T(8,128)(2,1)}), bf16[1408,2048]{1,0:T(8,128)(2,1)}) %all-gather.14.cloned.1.call-update) | async-done | bytes 5767184 | tf_op jit(solution)/shard_map/all_gather | solution.py:102
  428.0 15.5 %convolution_convert_fusion.1 = bf16[512,2048]{1,0:T(8,128)(2,1)} fusion(bf16[1408,2048]{1,0:T(8,128)(2,1)} %all-gather.14.cloned.1.call-done, bf16[512,2048]{1,0:T(8,128)(2,1)S(1)} %copy-done.6, bf16[2048,1408]{1,0:T(8,128)(2,1)} %all-gather.12.cloned.1.call-done, f32[512,1408]{1,0:T(8,128)} %fusion.39, f32[511,1408]{1,0:T(8,128)} %bitcast.24, ...), kind=kOutput, calls=%fused_computation.3 | convolution fusion | flops 5914558464 | bytes 24379392 | tf_op jit(solution)/shard_map/dot_general | solution.py:106
  443.6 29.5 %reduce-scatter.5.cloned.1.call-done = bf16[128,2048]{1,0:T(8,128)(2,1)} async-done(((bf16[512,2048]{1,0:T(8,128)(2,1)}), bf16[128,2048]{1,0:T(8,128)(2,1)}) %reduce-scatter.5.cloned.1.call-update) | async-done | bytes 524304 | tf_op jit(solution)/shard_map/reduce_scatter | solution.py:105
  473.0 1.3 fusion.11
  474.3 1.4 multiply_reduce_fusion
  475.7 2.1 multiply_convert_fusion
  (41 shorter events, 0.7 us)
Async XLA Ops:
  7.4 38.9 %copy-start.1 = (bf16[256,128]{1,0:T(8,128)(2,1)S(1)}, bf16[256,128]{1,0:T(8,128)(2,1)}, u32[]{:S(2)}) copy-start(bf16[256,128]{1,0:T(8,128)(2,1)} %param.13) | copy-start | bytes 196612
  7.4 70.4 %copy-start.2 = (bf16[128,256]{1,0:T(8,128)(2,1)S(1)}, bf16[128,256]{1,0:T(8,128)(2,1)}, u32[]{:S(2)}) copy-start(bf16[128,256]{1,0:T(8,128)(2,1)} %param.17) | copy-start | bytes 196612
  7.4 101.6 %all-gather.6.cloned.1.call-start = ((), (), s32[]{:S(2)}) async-start(), calls=%async_computation.2 | async-start | bytes 2621440 | tf_op jit(solution)/shard_map/all_gather | solution.py:52
  12.1 143.0 %reduce-scatter.3.cloned.1.call-start = ((), (), s32[]{:S(2)}) async-start(), calls=%async_computation.3 | async-start | bytes 2621440 | tf_op jit(solution)/shard_map/reduce_scatter | solution.py:83
  120.6 2.7 copy-start.4
  120.6 34.5 %copy-start = (bf16[128,2048]{1,0:T(8,128)(2,1)S(1)}, bf16[128,2048]{1,0:T(8,128)(2,1)}, u32[]{:S(2)}) copy-start(bf16[128,2048]{1,0:T(8,128)(2,1)} %param.12) | copy-start | bytes 1572868
  122.6 96.0 %all-gather.10.cloned.1.call-start = ((), (), s32[]{:S(2)}) async-start(), calls=%async_computation.5 | async-start | bytes 6488064 | tf_op jit(solution)/shard_map/all_gather | solution.py:96
  123.2 117.4 %all-gather.8.cloned.1.call-start = ((), (), s32[]{:S(2)}) async-start(), calls=%async_computation.4 | async-start | bytes 2621440 | tf_op jit(solution)/shard_map/all_gather | solution.py:94
  156.4 5.8 %copy-start.3 = (bf16[3,1408]{1,0:T(4,128)(2,1)S(1)}, bf16[3,1408]{1,0:T(4,128)(2,1)}, u32[]{:S(2)}) copy-start(bf16[3,1408]{1,0:T(4,128)(2,1)} %param.21) | copy-start | bytes 25348
  160.7 174.2 %all-gather.12.cloned.1.call-start = ((), (), s32[]{:S(2)}) async-start(), calls=%async_computation.6 | async-start | bytes 6488064 | tf_op jit(solution)/shard_map/all_gather | solution.py:97
  161.3 266.7 %all-gather.14.cloned.1.call-start = ((), (), s32[]{:S(2)}) async-start(), calls=%async_computation.7 | async-start | bytes 6488064 | tf_op jit(solution)/shard_map/all_gather | solution.py:102
  162.0 311.0 %reduce-scatter.5.cloned.1.call-start = ((), (), s32[]{:S(2)}) async-start(), calls=%async_computation.8 | async-start | bytes 2621440 | tf_op jit(solution)/shard_map/reduce_scatter | solution.py:105
  240.6 187.3 %copy-start.6 = (bf16[512,2048]{1,0:T(8,128)(2,1)S(1)}, bf16[512,2048]{1,0:T(8,128)(2,1)}, u32[]{:S(2)}) copy-start(bf16[512,2048]{1,0:T(8,128)(2,1)} %all-gather.8.cloned.1.call-done) | copy-start | bytes 6291460
  428.0 15.6 %copy-start.5 = (bf16[2048]{0:T(1024)(128)(2,1)S(1)}, bf16[2048]{0:T(1024)(128)(2,1)}, u32[]{:S(2)}) copy-start(bf16[2048]{0:T(1024)(128)(2,1)} %param.23) | copy-start | bytes 12292
Sparse Core Ops, SparseCore 0:
  12.2 25.2 all-gather.5
  122.8 32.3 reduce-scatter.2
  443.6 29.3 reduce-scatter.4
Sparse Core Ops, SparseCore 1:
  125.3 93.2 all-gather.9
  220.0 20.5 all-gather.7
  242.7 92.1 all-gather.11
  336.9 91.0 all-gather.13
where the time goes:
time: 486 us; the launch traced here: 485 us
  waiting for transfers between devices  320 us (66%)
  blocking collectives  102 us (21%)
  matrix products  31.6 us (7%)
  other arithmetic  16 us (3%)
  between operations  15 us (3%)
    all_gather x1, waiting for transfers between devices, shards(): whole_down = lax.all_gather(ffn_down, 'fs', axis=1, tiled=True)  93.1 us
    all_gather x1, waiting for transfers between devices, shards(): lax.all_gather(ffn_value, 'fs', axis=0, tiled=True)  85.8 us
    all_gather x1, waiting for transfers between devices, shards(): lax.all_gather(ffn_gate, 'fs', axis=0, tiled=True)  56.3 us
    all_gather x1, blocking collectives, shards(): lax.all_gather(signal_proj, 'fs', axis=0, tiled=True)  33.3 us
    reduce_scatter x1, waiting for transfers between devices, shards(): lax.psum_scatter(jnp.dot(selected, out_columns, preferred_element_type=jn...  31.8 us
    all_gather x1, blocking collectives, shards(): lax.all_gather(gate_proj, 'fs', axis=0, tiled=True)  31.5 us
    all_gather x1, blocking collectives, shards(): out_columns = lax.all_gather(mixer_out, 'fs', axis=1, tiled=True)  31.2 us
    reduce_scatter x1, waiting for transfers between devices, shards(): lax.psum_scatter(jnp.dot(selected, whole_down, preferred_element_type=jnp...  29.5 us
  transfers between devices with their start and end apart: 7, of which 6 were waited for; matrix products, arithmetic and copies ran while one was open for 3% of the time, Pallas kernels for 0%

commit v1 on v0

v1 whole, which is shorter than its diff:
```python
import functools
import math

import jax
import jax.numpy as jnp
from jax import lax
from jax.experimental import pallas as pl
from jax.experimental.pallas import tpu as pltpu
from jax.sharding import PartitionSpec as P

MIX_WIDTH = 512
HEAD_SIZE = 128
BLOCK = 128
SEGMENT = 64
LANES = 128
EPSILON = 1e-05
RESIDUAL_SCALE = math.sqrt(2.0)
MESH = pl.DeviceIdType.MESH
F32 = jnp.float32
BF16 = jnp.bfloat16


def normalize(values):
    row_mean = jnp.mean(values, axis=-1, keepdims=True)
    centred = values - row_mean
    spread = jnp.mean(centred * centred, axis=-1, keepdims=True)
    return centred * lax.rsqrt(spread + EPSILON)


def kernel(
    nz, ny, nx,
    tok, gs, mo, gv, dn, spatial, sgain, mgain, taps, ogain,
    out,
    gsb, mob, gvb, dnb, xin, stat, pm, prc, abm, pxr, mid, hin, hid, pb, rb, ab, xr, zb, zr,
    loc_sem, zs, zrs, ys, yrs, ts, trs,
):
    R, D = tok.shape
    C = mo.shape[0]
    cw = mo.shape[1]
    W = dn.shape[1]
    f = lax.axis_index("fs")
    t = lax.axis_index("tp")
    z, y = f // ny, f % ny
    x, c = t // 2, t % 2
    q = z % 2
    seq = nx * 2 * R

    def zpeer(d):
        return (lax.rem(z + d, nz) * ny + y, t)

    def ypeer(d):
        return (z * ny + lax.rem(y + d, ny), t)

    def xpeer(d):
        return (f, lax.rem(x + d, nx) * 2 + c)

    cpeer = (f, x * 2 + 1 - c)
    ppeer = ((z + 1 - 2 * q) * ny + y, t)

    def zsrc(d):
        return lax.rem(z + nz - d, nz)

    def ysrc(d):
        return lax.rem(y + ny - d, ny)

    def xsrc(d):
        return lax.rem(x + nx - d, nx)

    pending = []

    def send(src, dst, ssem, rsem, to):
        copy = pltpu.make_async_remote_copy(
            src_ref=src, dst_ref=dst, send_sem=ssem, recv_sem=rsem, device_id=to, device_id_type=MESH
        )
        copy.start()
        pending.append(copy)

    def arrived(dst, ssem, rsem, to):
        pltpu.make_async_remote_copy(
            src_ref=dst, dst_ref=dst, send_sem=ssem, recv_sem=rsem, device_id=to, device_id_type=MESH
        ).wait_recv()

    barrier = pltpu.get_barrier_semaphore()
    peers = [zpeer(d) for d in range(1, nz)] + [ypeer(d) for d in range(1, ny)]
    peers += [xpeer(d) for d in range(1, nx)] + [cpeer]
    for p in peers:
        pl.semaphore_signal(barrier, inc=1, device_id=p, device_id_type=MESH)
    pl.semaphore_wait(barrier, len(peers))

    bufs = (gsb, mob, gvb, dnb)

    def local(a, zz):
        return (gs, mo, gv.at[zz % 2], dn.at[zz % 2])[a]

    def issue(a):
        own = pltpu.make_async_copy(local(a, z), bufs[a].at[z, y], loc_sem.at[a])
        own.start()
        for d in range(1, nz):
            to = zpeer(d)
            send(local(a, lax.rem(z + d, nz)), bufs[a].at[z, y], zs.at[a, d], zrs.at[a, d], to)
        for e in range(1, ny):
            send(local(a, z), bufs[a].at[z, y], ys.at[a, 0, e], yrs.at[a, 0, e], ypeer(e))
        own.wait()

    def relay(a, d):
        zz = zsrc(d)
        arrived(bufs[a].at[zz, y], zs.at[a, d], zrs.at[a, d], zpeer(d))
        for e in range(1, ny):
            send(bufs[a].at[zz, y], bufs[a].at[zz, y], ys.at[a, d, e], yrs.at[a, d, e], ypeer(e))

    def complete(a, d):
        zz = zsrc(d)
        for e in range(1, ny):
            yy = ysrc(e)
            arrived(bufs[a].at[zz, yy], ys.at[a, d, e], yrs.at[a, d, e], ypeer(e))

    tslot = [0]

    def tsem():
        k = tslot[0]
        tslot[0] += 1
        return ts.at[k], trs.at[k]

    issue(0)
    issue(1)
    issue(2)

    xin[x, c] = normalize(tok[...].astype(F32)).astype(BF16)
    s1 = [tsem() for _ in range(nx)]
    s2 = [tsem() for _ in range(nx)]
    for d in range(1, nx):
        send(xin.at[x, c], xin.at[x, c], *s1[d], xpeer(d))
    send(xin.at[x, c], xin.at[x, c], *s2[0], cpeer)
    for a in (0, 1):
        for d in range(1, nz):
            relay(a, d)
    for d in range(1, nx):
        arrived(xin.at[xsrc(d), c], *s1[d], xpeer(d))
        send(xin.at[xsrc(d), c], xin.at[xsrc(d), c], *s2[d], cpeer)
    for d in range(nx):
        arrived(xin.at[xsrc(d), 1 - c], *s2[d], cpeer)
    for d in range(nz):
        complete(0, d)

    kdim = gs.shape[0]
    pre = jnp.dot(
        xin[...].reshape(seq, D), gsb[...].reshape(nz * ny * kdim, 2 * C), preferred_element_type=F32
    )
    branch_gate = jax.nn.gelu(pre[:, :C])
    branch_signal = jax.nn.gelu(pre[:, C:])
    total = jnp.sum(branch_signal, axis=1, keepdims=True)
    square = jnp.sum(branch_signal * branch_signal, axis=1, keepdims=True)
    lane = lax.broadcasted_iota(jnp.int32, (seq, LANES), 1)
    stat[0] = jnp.where(lane == 0, total, square).T[:8]
    sc = tsem()
    send(stat.at[0], stat.at[1], *sc, cpeer)
    arrived(stat.at[1], *sc, cpeer)
    stat[2] = stat[0] + stat[1]
    sx = [tsem() for _ in range(nx)]
    for d in range(1, nx):
        send(stat.at[2], stat.at[2 + d], *sx[d], xpeer(d))
    for d in range(1, nx):
        arrived(stat.at[2 + d], *sx[d], xpeer(d))
    summed = stat[2]
    for d in range(1, nx):
        summed = summed + stat[2 + d]
    back = summed.T
    row_mean = back[:, 0:1] / MIX_WIDTH
    spread = back[:, 1:2] / MIX_WIDTH - row_mean * row_mean
    spatial_input = (
        (branch_signal - row_mean) * lax.rsqrt(spread + EPSILON) * sgain[...].astype(F32)
    ).astype(BF16)
    rows_i = lax.broadcasted_iota(jnp.int32, (BLOCK, BLOCK), 0) // SEGMENT
    cols_i = lax.broadcasted_iota(jnp.int32, (BLOCK, BLOCK), 1) // SEGMENT
    own = spatial[t * C // HEAD_SIZE]
    own = jnp.where(cols_i <= rows_i, own, jnp.zeros_like(own))
    for d in range(nz):
        complete(1, d)
    per = BLOCK // R if R < BLOCK else 1
    gated = jnp.concatenate(
        [
            branch_gate[b * BLOCK:(b + 1) * BLOCK]
            * jnp.dot(own, spatial_input[b * BLOCK:(b + 1) * BLOCK], preferred_element_type=F32)
            for b in range(seq // BLOCK)
        ],
        axis=0,
    ).astype(BF16)
    for k in range(nz * ny):
        part = jnp.dot(gated, mob[k // ny, k % ny], preferred_element_type=F32).astype(BF16)
        for b in range(nx * 2):
            pm[b % 2, b // 2, :, k * cw:(k + 1) * cw] = part[b * R:(b + 1) * R]
    sc = tsem()
    send(pm.at[1 - c], prc, *sc, cpeer)
    arrived(prc, *sc, cpeer)
    for b in range(nx):
        abm[b] = (pm[c, b].astype(F32) + prc[b].astype(F32)).astype(BF16)
    sx = [tsem() for _ in range(nx)]
    for d in range(1, nx):
        send(abm.at[lax.rem(x + d, nx)], pxr.at[d - 1], *sx[d], xpeer(d))
    relay(2, 1)
    for d in range(1, nx):
        arrived(pxr.at[d - 1], *sx[d], xpeer(d))
    mix_out = pm[c, x].astype(F32) + prc[x].astype(F32)
    for d in range(1, nx):
        mix_out = mix_out + pxr[d - 1].astype(F32)
    mid[...] = (
        normalize(RESIDUAL_SCALE * tok[...].astype(F32) + mix_out) * mgain[...].astype(F32)
    ).astype(BF16)
    hin[q, x, c] = normalize(mid[...].astype(F32)).astype(BF16)

    sp = tsem()
    send(hin.at[q, x, c], hin.at[q, x, c], *sp, ppeer)
    sx = [[tsem() for _ in range(nx)] for _ in range(2)]
    sy = [[tsem() for _ in range(nx)] for _ in range(2)]
    for d in range(1, nx):
        send(hin.at[q, x, c], hin.at[q, x, c], *sx[0][d], xpeer(d))
    send(hin.at[q, x, c], hin.at[q, x, c], *sy[0][0], cpeer)
    issue(3)
    for d in range(2, nz):
        relay(2, d)
    arrived(hin.at[1 - q, x, c], *sp, ppeer)
    for d in range(1, nx):
        send(hin.at[1 - q, x, c], hin.at[1 - q, x, c], *sx[1][d], xpeer(d))
    send(hin.at[1 - q, x, c], hin.at[1 - q, x, c], *sy[1][0], cpeer)
    for k, s in enumerate((q, 1 - q)):
        for d in range(1, nx):
            arrived(hin.at[s, xsrc(d), c], *sx[k][d], xpeer(d))
            send(hin.at[s, xsrc(d), c], hin.at[s, xsrc(d), c], *sy[k][d], cpeer)
    for k, s in enumerate((q, 1 - q)):
        for d in range(nx):
            arrived(hin.at[s, xsrc(d), 1 - c], *sy[k][d], cpeer)
    for d in range(nz):
        complete(2, d)

    for s in range(2):

        def column(j, carry):
            at = pl.multiple_of(j * LANES, LANES)
            at_v = pl.multiple_of(W + j * LANES, LANES)
            lhs = hin[s].reshape(seq, D)
            wg = gvb[:, :, :, pl.ds(at, LANES)].reshape(D, LANES)
            wv = gvb[:, :, :, pl.ds(at_v, LANES)].reshape(D, LANES)
            both = jnp.dot(lhs, jnp.concatenate([wg, wv], axis=1), preferred_element_type=F32)
            gate = both[:, :LANES]
            value = both[:, LANES:]
            tap = taps[:, pl.ds(at, LANES)].astype(F32)
            row = lax.broadcasted_iota(jnp.int32, gate.shape, 0)
            one = jnp.where(row >= 1, pltpu.roll(gate, 1, 0), 0.0)
            two = jnp.where(row >= 2, pltpu.roll(gate, 2, 0), 0.0)
            conv = tap[0:1] * two + tap[1:2] * one + tap[2:3] * gate
            hid[s, :, pl.ds(at, LANES)] = (jax.nn.silu(conv) * value).astype(BF16)
            return carry

        lax.fori_loop(0, W // LANES, column, 0)

    sc = [tsem() for _ in range(nz)]
    sx = [[tsem() for _ in range(nx)] for _ in range(nz)]
    sz = [tsem() for _ in range(nz)]

    def down(i):
        g = zsrc(i)
        for s in range(2):
            for yy in range(ny):
                part = jnp.dot(hid[s], dnb[g, yy], preferred_element_type=F32).astype(BF16)
                for b in range(nx * 2):
                    pb[b % 2, g, b // 2, s, :, yy * cw:(yy + 1) * cw] = part[b * R:(b + 1) * R]
        send(pb.at[1 - c, g], rb.at[i], *sc[i], cpeer)

    def over_x(i):
        g = zsrc(i)
        arrived(rb.at[i], *sc[i], cpeer)
        for b in range(nx):
            for s in range(2):
                ab[i, b, s] = (pb[c, g, b, s].astype(F32) + rb[i, b, s].astype(F32)).astype(BF16)
        for d in range(1, nx):
            send(ab.at[i, lax.rem(x + d, nx)], xr.at[i, d - 1], *sx[i][d], xpeer(d))

    def over_z(i):
        g = zsrc(i)
        for d in range(1, nx):
            arrived(xr.at[i, d - 1], *sx[i][d], xpeer(d))
        for s in range(2):
            acc = ab[i, x, s].astype(F32)
            for d in range(1, nx):
                acc = acc + xr[i, d - 1, s].astype(F32)
            zb[g, s] = acc.astype(BF16)

    for d in range(1, nz):
        relay(3, d)
    for i in range(nz):
        complete(3, i)
        down(i)
        if i >= 1:
            over_x(i - 1)
        if i >= 2:
            over_z(i - 2)
    over_x(nz - 1)
    over_z(nz - 2)
    over_z(nz - 1)
    for g in range(nz):
        send(zb.at[g, 1 - q], zr.at[g], *sz[g], ppeer)
    for g in range(nz):
        arrived(zr.at[g], *sz[g], ppeer)
    ffn_out = jnp.concatenate(
        [zb[g, q].astype(F32) + zr[g].astype(F32) for g in range(nz)], axis=1
    )
    out[...] = (
        normalize(RESIDUAL_SCALE * mid[...].astype(F32) + ffn_out) * ogain[...].astype(F32)
    ).astype(BF16)
    for copy in pending:
        copy.wait_send()


def shards(nf, nt, ny, tokens, gate_proj, signal_proj, spatial, signal_gain, mixer_out, mixer_gain, ffn_gate, ffn_value, conv_taps, ffn_down, output_gain):
    nz = nf // ny
    nx = nt // 2
    R, D = tokens.shape
    C = gate_proj.shape[1]
    H = ffn_gate.shape[1]
    W = -(-H // (2 * LANES)) * LANES
    cw = mixer_out.shape[1]
    seq = nx * 2 * R
    q = (lax.axis_index("fs") // ny) % 2

    gs = jnp.concatenate([gate_proj, signal_proj], axis=1)
    gv = jnp.stack(
        [
            jnp.concatenate([ffn_gate[:, :W], ffn_value[:, :W]], axis=1),
            jnp.concatenate([ffn_gate[:, H - W:], ffn_value[:, H - W:]], axis=1),
        ]
    )
    fresh = (jnp.arange(W) >= 2 * W - H)[:, None]
    low = ffn_down[H - W:]
    dn = jnp.stack([ffn_down[:W], jnp.where(fresh, low, jnp.zeros_like(low))])
    taps = lax.dynamic_slice_in_dim(conv_taps, q * (H - W), W, 1)
    gw = ny * cw
    vm = functools.partial(pltpu.VMEM)
    dma = pltpu.SemaphoreType.DMA
    n_t = 2 * nx + 1 + nx + 1 + nx + 1 + 4 * nx + nz * (2 + nx)
    scratch = [
        vm((nz, ny) + gs.shape, BF16),
        vm((nz, ny) + mixer_out.shape, BF16),
        vm((nz, ny) + gv.shape[1:], BF16),
        vm((nz, ny) + dn.shape[1:], BF16),
        vm((nx, 2, R, D), BF16),
        vm((2 + nx, 8, seq), F32),
        vm((2, nx, R, D), BF16),
        vm((nx, R, D), BF16),
        vm((nx, R, D), BF16),
        vm((nx - 1, R, D), BF16),
        vm((R, D), BF16),
        vm((2, nx, 2, R, D), BF16),
        vm((2, seq, W), BF16),
        vm((2, nz, nx, 2, R, gw), BF16),
        vm((nz, nx, 2, R, gw), BF16),
        vm((nz, nx, 2, R, gw), BF16),
        vm((nz, nx - 1, 2, R, gw), BF16),
        vm((nz, 2, R, gw), BF16),
        vm((nz, R, gw), BF16),
        dma((4,)),
        dma((4, nz)),
        dma((4, nz)),
        dma((4, nz, ny)),
        dma((4, nz, ny)),
        dma((n_t,)),
        dma((n_t,)),
    ]
    return pl.pallas_call(
        functools.partial(kernel, nz, ny, nx),
        out_shape=jax.ShapeDtypeStruct((R, D), BF16),
        in_specs=[pl.BlockSpec(memory_space=pltpu.VMEM)] * 10,
        out_specs=pl.BlockSpec(memory_space=pltpu.VMEM),
        scratch_shapes=scratch,
        compiler_params=pltpu.CompilerParams(
            collective_id=0, has_side_effects=True, vmem_limit_bytes=67043328
        ),
    )(
        tokens, gs, mixer_out, gv, dn, spatial, signal_gain[None], mixer_gain[None], taps, output_gain[None]
    )


def solution(mesh):
    nf, nt = mesh.shape["fs"], mesh.shape["tp"]
    ny = 2 ** (int(math.log2(nf // 2)) // 2)
    in_specs = (
        P(("fs", "tp"), None),
        P("fs", "tp"),
        P("fs", "tp"),
        P(),
        P("tp"),
        P("tp", "fs"),
        P(),
        P("fs", "tp"),
        P("fs", "tp"),
        P(None, "tp"),
        P("tp", "fs"),
        P(),
    )
    return jax.shard_map(
        functools.partial(shards, nf, nt, ny),
        mesh=mesh,
        in_specs=in_specs,
        out_specs=P(("fs", "tp"), None),
        check_vma=False,
    )
```

time: 486 us -> 205 us (0.42)
  waiting for transfers between devices: 320 us -> 0 us
  Pallas kernels: 0 us -> 196 us
  blocking collectives: 102 us -> 0 us
  matrix products: 31.6 us -> 0 us
  between operations: 15 us -> 0.08 us
  other arithmetic: 16 us -> 3.19 us
  local copies, waits for them, and re-layouts: 0.08 us -> 5.69 us
    all_gather x5 -> x0, waiting for transfers between devices: 257 us -> none  [the longest x1 93.1 us: shards(): whole_down = lax.all_gather(ffn_down, 'fs', axis=1, tiled=True)]
    pallas_call x0 -> x1, Pallas kernels: none -> 196 us  [shards(): pl.pallas_call(functools.partial(kernel, nz, ny, nx), out_shape=jax.Shape...]
    all_gather x3 -> x0, blocking collectives: 96 us -> none  [the longest x1 33.3 us: shards(): lax.all_gather(signal_proj, 'fs', axis=0, tiled=True)]
    reduce_scatter x2 -> x0, waiting for transfers between devices: 61.3 us -> none  [the longest x1 31.8 us: shards(): lax.psum_scatter(jnp.dot(selected, out_columns, preferred_element_type=jn...]
    dot_general x6 -> x0, matrix products: 31.6 us -> none  [the longest x1 15.5 us: shards(): jnp.dot(selected, whole_down, preferred_element_type=jnp.float32)]
    reduce_sum x8 -> x0, other arithmetic: 9.61 us -> none  [the longest x4 5.26 us: normalize(): row_mean = jnp.mean(values, axis=-1, keepdims=True)]
    convert_element_type x8 -> x0, other arithmetic: 6.28 us -> none  [the longest x1 2.15 us: shards(): mix_input = normalize(residual).astype(jnp.bfloat16)]
    psum x1 -> x0, blocking collectives: 5.66 us -> none  [shards(): lax.psum((jnp.sum(branch_signal, axis=1), jnp.sum(branch_signal * branch_...]
  transfers between devices with their start and end apart: 7 -> 0, of which waited for: 6 -> 0; matrix products, arithmetic and copies ran while one was open for 3% -> 0% of each run, Pallas kernels for 0% -> 0%
where the time goes in v1:
time: 205 us
  Pallas kernels  196 us (96%)
  local copies, waits for them, and re-layouts  5.69 us (3%)
  other arithmetic  3.19 us (2%)
    pallas_call x1, Pallas kernels, shards(): pl.pallas_call(functools.partial(kernel, nz, ny, nx), out_shape=jax.Shape...  196 us

profile of v1, /device:TPU:0, one launch (start us, length us, event | category | flops | bytes accessed | tf_op | source)
XLA Modules:
  0.0 204.6 jit_solution(8975954741465250788)
XLA Ops:
  0.0 0.0 copy-start
  0.0 1.4 constant_dynamic-slice_fusion.taps
  1.4 1.2 fusion.1
  2.5 0.0 copy-done
  2.5 0.1 fusion
  2.6 0.1 maximum_bitcast_fusion
  2.7 0.0 copy-start.1
  2.7 1.3 pad_maximum_fusion.gv
  4.0 0.0 copy-done.1
  4.0 0.0 copy-start.2
  4.0 0.0 copy-start.3
  4.0 0.0 copy-start.4
  4.1 0.0 copy-start.5
  4.1 0.2 slice_bitcast_fusion
  4.2 0.9 pad_maximum_fusion.1.dn
  5.2 0.0 copy-done.2
  5.2 0.0 copy-done.3
  5.2 0.7 pad_maximum_fusion.2.gs
  5.9 0.0 copy-done.4
  5.9 0.6 broadcast_in_dim.24.mgain
  6.5 0.0 copy-done.5
  6.5 0.6 broadcast_in_dim.25.ogain
  7.1 195.6 %shard_map.118 = bf16[128,2048]{1,0:T(8,128)(2,1)} custom-call(bf16[128,2048]{1,0:T(8,128)(2,1)} %tok.1, bf16[256,256]{1,0:T(8,128)(2,1)} %pad_maximum_fusion.2.gs, bf16[128,256]{1,0:T(8,128)(2,1)} %mo.1, bf16[2,256,1536]{2,1,0:T(8,128)(2,1)} %pad_maximum_fusion.gv, bf16[2,768,256]{2,1,0:T(8,128)(2,1)} %pad_maximum_fusion.1.dn, ...), custom_call_target="tpu_custom_call" | custom-call | tf_op jit(solution)/shard_map/pallas_call | solution.py:368
  202.7 1.9 copy.14
  (1 shorter events, 0.0 us)
Async XLA Ops:
  0.0 2.5 %copy-start = (bf16[256,1408]{1,0:T(8,128)(2,1)S(1)}, bf16[256,1408]{1,0:T(8,128)(2,1)}, u32[]{:S(2)}) copy-start(bf16[256,1408]{1,0:T(8,128)(2,1)} %param.19) | copy-start | bytes 2162692
  2.7 1.3 copy-start.1
  4.0 1.2 copy-start.2
  4.0 1.2 copy-start.3
  4.0 1.8 copy-start.4
  4.1 2.4 %copy-start.5 = (bf16[2048]{0:T(1024)(128)(2,1)S(1)}, bf16[2048]{0:T(1024)(128)(2,1)}, u32[]{:S(2)}) copy-start(bf16[2048]{0:T(1024)(128)(2,1)} %param.23) | copy-start | bytes 12292

commit v2 on v1

--- a/solution.py
+++ b/solution.py
@@ -13,6 +13,8 @@
 BLOCK = 128
 SEGMENT = 64
 LANES = 128
+GV_PIECES = 4
+DN_PIECES = 2
 EPSILON = 1e-05
 RESIDUAL_SCALE = math.sqrt(2.0)
 MESH = pl.DeviceIdType.MESH
@@ -87,32 +89,53 @@
         pl.semaphore_signal(barrier, inc=1, device_id=p, device_id_type=MESH)
     pl.semaphore_wait(barrier, len(peers))
 
-    bufs = (gsb, mob, gvb, dnb)
+    gv_rows = gv.shape[1] // GV_PIECES
+    dn_rows = W // DN_PIECES
+    DN = 2 + GV_PIECES
+    EARLY = DN - 2
+
+    def slot(a, zz, yy):
+        if a == 0:
+            return gsb.at[zz, yy]
+        if a == 1:
+            return mob.at[zz, yy]
+        if a < DN:
+            return gvb.at[zz, yy, pl.ds((a - 2) * gv_rows, gv_rows)]
+        return dnb.at[zz, yy, pl.ds((a - DN) * dn_rows, dn_rows)]
 
     def local(a, zz):
-        return (gs, mo, gv.at[zz % 2], dn.at[zz % 2])[a]
+        if a == 0:
+            return gs
+        if a == 1:
+            return mo
+        if a < DN:
+            return gv.at[zz % 2, pl.ds((a - 2) * gv_rows, gv_rows)]
+        return dn.at[zz % 2, pl.ds((a - DN) * dn_rows, dn_rows)]
 
     def issue(a):
-        own = pltpu.make_async_copy(local(a, z), bufs[a].at[z, y], loc_sem.at[a])
+        own = pltpu.make_async_copy(local(a, z), slot(a, z, y), loc_sem.at[a])
         own.start()
         for d in range(1, nz):
             to = zpeer(d)
-            send(local(a, lax.rem(z + d, nz)), bufs[a].at[z, y], zs.at[a, d], zrs.at[a, d], to)
+            send(local(a, lax.rem(z + d, nz)), slot(a, z, y), zs.at[a, d], zrs.at[a, d], to)
         for e in range(1, ny):
-            send(local(a, z), bufs[a].at[z, y], ys.at[a, 0, e], yrs.at[a, 0, e], ypeer(e))
+            send(local(a, z), slot(a, z, y), ys.at[a, 0, e], yrs.at[a, 0, e], ypeer(e))
         own.wait()
 
-    def relay(a, d):
-        zz = zsrc(d)
-        arrived(bufs[a].at[zz, y], zs.at[a, d], zrs.at[a, d], zpeer(d))
-        for e in range(1, ny):
-            send(bufs[a].at[zz, y], bufs[a].at[zz, y], ys.at[a, d, e], yrs.at[a, d, e], ypeer(e))
+    def relay(a):
+        for d in range(1, nz):
+            zz = zsrc(d)
+            arrived(slot(a, zz, y), zs.at[a, d], zrs.at[a, d], zpeer(d))
+            for e in range(1, ny):
+                send(slot(a, zz, y), slot(a, zz, y), ys.at[a, d, e], yrs.at[a, d, e], ypeer(e))
 
     def complete(a, d):
         zz = zsrc(d)
         for e in range(1, ny):
             yy = ysrc(e)
-            arrived(bufs[a].at[zz, yy], ys.at[a, d, e], yrs.at[a, d, e], ypeer(e))
+            arrived(slot(a, zz, yy), ys.at[a, d, e], yrs.at[a, d, e], ypeer(e))
+
+    scope = jax.named_scope
 
     tslot = [0]
 
@@ -123,7 +146,6 @@
 
     issue(0)
     issue(1)
-    issue(2)
 
     xin[x, c] = normalize(tok[...].astype(F32)).astype(BF16)
     s1 = [tsem() for _ in range(nx)]
@@ -131,16 +153,19 @@
     for d in range(1, nx):
         send(xin.at[x, c], xin.at[x, c], *s1[d], xpeer(d))
     send(xin.at[x, c], xin.at[x, c], *s2[0], cpeer)
-    for a in (0, 1):
-        for d in range(1, nz):
-            relay(a, d)
+    with scope("relay_mix"):
+        relay(0)
+        relay(1)
+    for a in range(2, EARLY):
+        issue(a)
     for d in range(1, nx):
         arrived(xin.at[xsrc(d), c], *s1[d], xpeer(d))
         send(xin.at[xsrc(d), c], xin.at[xsrc(d), c], *s2[d], cpeer)
     for d in range(nx):
         arrived(xin.at[xsrc(d), 1 - c], *s2[d], cpeer)
-    for d in range(nz):
-        complete(0, d)
+    with scope("complete_gs"):
+        for d in range(nz):
+            complete(0, d)
 
     kdim = gs.shape[0]
     pre = jnp.dot(
@@ -174,9 +199,9 @@
     cols_i = lax.broadcasted_iota(jnp.int32, (BLOCK, BLOCK), 1) // SEGMENT
     own = spatial[t * C // HEAD_SIZE]
     own = jnp.where(cols_i <= rows_i, own, jnp.zeros_like(own))
-    for d in range(nz):
-        complete(1, d)
-    per = BLOCK // R if R < BLOCK else 1
+    with scope("complete_mo"):
+        for d in range(nz):
+            complete(1, d)
     gated = jnp.concatenate(
         [
             branch_gate[b * BLOCK:(b + 1) * BLOCK]
@@ -197,9 +222,9 @@
     sx = [tsem() for _ in range(nx)]
     for d in range(1, nx):
         send(abm.at[lax.rem(x + d, nx)], pxr.at[d - 1], *sx[d], xpeer(d))
-    relay(2, 1)
-    for d in range(1, nx):
-        arrived(pxr.at[d - 1], *sx[d], xpeer(d))
+    with scope("mix_x"):
+        for d in range(1, nx):
+            arrived(pxr.at[d - 1], *sx[d], xpeer(d))
     mix_out = pm[c, x].astype(F32) + prc[x].astype(F32)
     for d in range(1, nx):
         mix_out = mix_out + pxr[d - 1].astype(F32)
@@ -215,22 +240,33 @@
     for d in range(1, nx):
         send(hin.at[q, x, c], hin.at[q, x, c], *sx[0][d], xpeer(d))
     send(hin.at[q, x, c], hin.at[q, x, c], *sy[0][0], cpeer)
-    issue(3)
-    for d in range(2, nz):
-        relay(2, d)
-    arrived(hin.at[1 - q, x, c], *sp, ppeer)
+    for a in range(EARLY, DN + DN_PIECES):
+        issue(a)
+    for a in range(2, DN - 1):
+        with scope(f"relay_gv{a - 2}"):
+            relay(a)
+    with scope("relay_gv3"):
+        relay(DN - 1)
+    with scope("pair_rows"):
+        arrived(hin.at[1 - q, x, c], *sp, ppeer)
     for d in range(1, nx):
         send(hin.at[1 - q, x, c], hin.at[1 - q, x, c], *sx[1][d], xpeer(d))
     send(hin.at[1 - q, x, c], hin.at[1 - q, x, c], *sy[1][0], cpeer)
-    for k, s in enumerate((q, 1 - q)):
-        for d in range(1, nx):
-            arrived(hin.at[s, xsrc(d), c], *sx[k][d], xpeer(d))
-            send(hin.at[s, xsrc(d), c], hin.at[s, xsrc(d), c], *sy[k][d], cpeer)
-    for k, s in enumerate((q, 1 - q)):
-        for d in range(nx):
-            arrived(hin.at[s, xsrc(d), 1 - c], *sy[k][d], cpeer)
-    for d in range(nz):
-        complete(2, d)
+    with scope("rows_x"):
+        for k, s in enumerate((q, 1 - q)):
+            for d in range(1, nx):
+                arrived(hin.at[s, xsrc(d), c], *sx[k][d], xpeer(d))
+                send(hin.at[s, xsrc(d), c], hin.at[s, xsrc(d), c], *sy[k][d], cpeer)
+    with scope("rows_core"):
+        for k, s in enumerate((q, 1 - q)):
+            for d in range(nx):
+                arrived(hin.at[s, xsrc(d), 1 - c], *sy[k][d], cpeer)
+    with scope("relay_dn0"):
+        relay(DN)
+    with scope("complete_gv"):
+        for a in range(2, DN):
+            for d in range(nz):
+                complete(a, d)
 
     for s in range(2):
 
@@ -243,7 +279,7 @@
             both = jnp.dot(lhs, jnp.concatenate([wg, wv], axis=1), preferred_element_type=F32)
             gate = both[:, :LANES]
             value = both[:, LANES:]
-            tap = taps[:, pl.ds(at, LANES)].astype(F32)
+            tap = taps[q, :, pl.ds(at, LANES)].astype(F32)
             row = lax.broadcasted_iota(jnp.int32, gate.shape, 0)
             one = jnp.where(row >= 1, pltpu.roll(gate, 1, 0), 0.0)
             two = jnp.where(row >= 2, pltpu.roll(gate, 2, 0), 0.0)
@@ -251,56 +287,66 @@
             hid[s, :, pl.ds(at, LANES)] = (jax.nn.silu(conv) * value).astype(BF16)
             return carry
 
-        lax.fori_loop(0, W // LANES, column, 0)
-
-    sc = [tsem() for _ in range(nz)]
-    sx = [[tsem() for _ in range(nx)] for _ in range(nz)]
-    sz = [tsem() for _ in range(nz)]
+        with scope("gate_value"):
+            lax.fori_loop(0, W // LANES, column, 0)
+        if s == 0:
+            with scope("relay_dn1"):
+                for a in range(DN + 1, DN + DN_PIECES):
+                    relay(a)
+
+    sc = [[tsem() for _ in range(2)] for _ in range(nz)]
+    sx = [[[tsem() for _ in range(nx)] for _ in range(2)] for _ in range(nz)]
+    zbase = tslot[0]
+    tslot[0] += nz
+    turns = (1 - q, q)
 
     def down(i):
         g = zsrc(i)
-        for s in range(2):
+        for k, s in enumerate(turns):
             for yy in range(ny):
                 part = jnp.dot(hid[s], dnb[g, yy], preferred_element_type=F32).astype(BF16)
                 for b in range(nx * 2):
-                    pb[b % 2, g, b // 2, s, :, yy * cw:(yy + 1) * cw] = part[b * R:(b + 1) * R]
-        send(pb.at[1 - c, g], rb.at[i], *sc[i], cpeer)
+                    pb[b % 2, g, s, b // 2, :, yy * cw:(yy + 1) * cw] = part[b * R:(b + 1) * R]
+            send(pb.at[1 - c, g, s], rb.at[i, s], *sc[i][k], cpeer)
 
     def over_x(i):
         g = zsrc(i)
-        arrived(rb.at[i], *sc[i], cpeer)
-        for b in range(nx):
-            for s in range(2):
-                ab[i, b, s] = (pb[c, g, b, s].astype(F32) + rb[i, b, s].astype(F32)).astype(BF16)
-        for d in range(1, nx):
-            send(ab.at[i, lax.rem(x + d, nx)], xr.at[i, d - 1], *sx[i][d], xpeer(d))
+        for k, s in enumerate(turns):
+            arrived(rb.at[i, s], *sc[i][k], cpeer)
+            for b in range(nx):
+                ab[i, s, b] = (pb[c, g, s, b].astype(F32) + rb[i, s, b].astype(F32)).astype(BF16)
+            for d in range(1, nx):
+                send(ab.at[i, s, lax.rem(x + d, nx)], xr.at[i, d - 1, s], *sx[i][k][d], xpeer(d))
 
     def over_z(i):
         g = zsrc(i)
-        for d in range(1, nx):
-            arrived(xr.at[i, d - 1], *sx[i][d], xpeer(d))
-        for s in range(2):
-            acc = ab[i, x, s].astype(F32)
+        for k, s in enumerate(turns):
+            for d in range(1, nx):
+                arrived(xr.at[i, d - 1, s], *sx[i][k][d], xpeer(d))
+            acc = ab[i, s, x].astype(F32)
             for d in range(1, nx):
                 acc = acc + xr[i, d - 1, s].astype(F32)
             zb[g, s] = acc.astype(BF16)
-
-    for d in range(1, nz):
-        relay(3, d)
+            if k == 0:
+                send(zb.at[g, s], zr.at[g], ts.at[zbase + g], trs.at[zbase + g], ppeer)
+
     for i in range(nz):
-        complete(3, i)
-        down(i)
+        with scope(f"complete_dn{i}"):
+            for a in range(DN, DN + DN_PIECES):
+                complete(a, i)
+        with scope(f"down{i}"):
+            down(i)
         if i >= 1:
             over_x(i - 1)
         if i >= 2:
             over_z(i - 2)
-    over_x(nz - 1)
-    over_z(nz - 2)
-    over_z(nz - 1)
-    for g in range(nz):
-        send(zb.at[g, 1 - q], zr.at[g], *sz[g], ppeer)
-    for g in range(nz):
-        arrived(zr.at[g], *sz[g], ppeer)
+    with scope("tail_x"):
+        over_x(nz - 1)
+        over_z(nz - 2)
+        over_z(nz - 1)
+    with scope("tail_z"):
+        for g in range(nz):
+            arrived(zr.at[g], ts.at[zbase + g], trs.at[zbase + g], ppeer)
     ffn_out = jnp.concatenate(
         [zb[g, q].astype(F32) + zr[g].astype(F32) for g in range(nz)], axis=1
     )
@@ -320,7 +366,6 @@
     W = -(-H // (2 * LANES)) * LANES
     cw = mixer_out.shape[1]
     seq = nx * 2 * R
-    q = (lax.axis_index("fs") // ny) % 2
 
     gs = jnp.concatenate([gate_proj, signal_proj], axis=1)
     gv = jnp.stack(
@@ -332,11 +377,12 @@
     fresh = (jnp.arange(W) >= 2 * W - H)[:, None]
     low = ffn_down[H - W:]
     dn = jnp.stack([ffn_down[:W], jnp.where(fresh, low, jnp.zeros_like(low))])
-    taps = lax.dynamic_slice_in_dim(conv_taps, q * (H - W), W, 1)
+    taps = jnp.stack([conv_taps[:, :W], conv_taps[:, H - W:]])
     gw = ny * cw
-    vm = functools.partial(pltpu.VMEM)
+    vm = pltpu.VMEM
+    n_w = 2 + GV_PIECES + DN_PIECES
     dma = pltpu.SemaphoreType.DMA
-    n_t = 2 * nx + 1 + nx + 1 + nx + 1 + 4 * nx + nz * (2 + nx)
+    n_t = 2 * nx + 1 + nx + 1 + nx + 1 + 4 * nx + nz * (3 + 2 * nx)
     scratch = [
         vm((nz, ny) + gs.shape, BF16),
         vm((nz, ny) + mixer_out.shape, BF16),
@@ -351,17 +397,17 @@
         vm((R, D), BF16),
         vm((2, nx, 2, R, D), BF16),
         vm((2, seq, W), BF16),
-        vm((2, nz, nx, 2, R, gw), BF16),
-        vm((nz, nx, 2, R, gw), BF16),
-        vm((nz, nx, 2, R, gw), BF16),
+        vm((2, nz, 2, nx, R, gw), BF16),
+        vm((nz, 2, nx, R, gw), BF16),
+        vm((nz, 2, nx, R, gw), BF16),
         vm((nz, nx - 1, 2, R, gw), BF16),
         vm((nz, 2, R, gw), BF16),
         vm((nz, R, gw), BF16),
-        dma((4,)),
-        dma((4, nz)),
-        dma((4, nz)),
-        dma((4, nz, ny)),
-        dma((4, nz, ny)),
+        dma((n_w,)),
+        dma((n_w, nz)),
+        dma((n_w, nz)),
+        dma((n_w, nz, ny)),
+        dma((n_w, nz, ny)),
         dma((n_t,)),
         dma((n_t,)),
     ]

time: 205 us -> 178 us (0.87)
  Pallas kernels: 196 us -> 169 us
    pallas_call x1, Pallas kernels: 196 us -> 169 us  [shards(): pl.pallas_call(functools.partial(kernel, nz, ny, nx), out_shape=jax.Shape...]
where the time goes in v2:
time: 178 us; the launch traced here: 177 us
  Pallas kernels  169 us (95%)
  local copies, waits for them, and re-layouts  4.51 us (3%)
  other arithmetic  3.8 us (2%)
    pallas_call x1, Pallas kernels, shards(): pl.pallas_call(functools.partial(kernel, nz, ny, nx), out_shape=jax.Shape...  169 us

profile of v2, /device:TPU:0, one launch (start us, length us, event | category | flops | bytes accessed | tf_op | source)
XLA Modules:
  0.0 177.0 jit_solution(4960967900465220113)
XLA Ops:
  0.0 0.0 copy-start
  0.0 1.2 fusion.1
  1.2 0.1 copy-done
  1.3 0.1 fusion
  1.4 0.1 maximum_bitcast_fusion
  1.5 0.0 copy-start.1
  1.5 1.3 pad_maximum_fusion.gv
  2.8 0.0 copy-done.1
  2.8 0.0 copy-start.4
  2.8 0.0 copy-start.2
  2.9 0.0 copy-start.3
  2.9 0.0 copy-start.5
  2.9 0.0 copy-start.6
  2.9 0.2 slice_bitcast_fusion
  3.1 0.9 pad_maximum_fusion.1.dn
  4.0 0.0 copy-done.4
  4.0 0.6 pad_maximum_fusion.3.taps
  4.6 0.0 copy-done.2
  4.6 0.0 copy-done.3
  4.6 0.7 pad_maximum_fusion.2.gs
  5.3 0.0 copy-done.5
  5.3 0.6 broadcast_in_dim.24.mgain
  5.9 0.0 copy-done.6
  5.9 0.6 broadcast_in_dim.25.ogain
  6.5 168.6 %shard_map.118 = bf16[128,2048]{1,0:T(8,128)(2,1)} custom-call(bf16[128,2048]{1,0:T(8,128)(2,1)} %tok.1, bf16[256,256]{1,0:T(8,128)(2,1)} %pad_maximum_fusion.2.gs, bf16[128,256]{1,0:T(8,128)(2,1)} %mo.1, bf16[2,256,1536]{2,1,0:T(8,128)(2,1)} %pad_maximum_fusion.gv, bf16[2,768,256]{2,1,0:T(8,128)(2,1)} %pad_maximum_fusion.1.dn, ...), custom_call_target="tpu_custom_call" | custom-call | tf_op jit(solution)/shard_map/pallas_call | solution.py:414
  175.1 1.9 %copy.14 = bf16[128,2048]{1,0:T(8,128)(2,1)} copy(bf16[128,2048]{1,0:T(8,128)(2,1)} %shard_map.118) | data formatting | bytes 1048576
  (2 shorter events, 0.0 us)
Async XLA Ops:
  0.0 1.3 copy-start
  1.5 1.3 copy-start.1
  2.8 1.2 copy-start.4
  2.8 1.8 %copy-start.2 = (bf16[256,128]{1,0:T(8,128)(2,1)S(1)}, bf16[256,128]{1,0:T(8,128)(2,1)}, u32[]{:S(2)}) copy-start(bf16[256,128]{1,0:T(8,128)(2,1)} %param.14) | copy-start | bytes 196612
  2.9 1.8 %copy-start.3 = (bf16[256,128]{1,0:T(8,128)(2,1)S(1)}, bf16[256,128]{1,0:T(8,128)(2,1)}, u32[]{:S(2)}) copy-start(bf16[256,128]{1,0:T(8,128)(2,1)} %param.13) | copy-start | bytes 196612
  2.9 2.4 %copy-start.5 = (bf16[2048]{0:T(1024)(128)(2,1)S(1)}, bf16[2048]{0:T(1024)(128)(2,1)}, u32[]{:S(2)}) copy-start(bf16[2048]{0:T(1024)(128)(2,1)} %param.18) | copy-start | bytes 12292
  2.9 3.0 %copy-start.6 = (bf16[2048]{0:T(1024)(128)(2,1)S(1)}, bf16[2048]{0:T(1024)(128)(2,1)}, u32[]{:S(2)}) copy-start(bf16[2048]{0:T(1024)(128)(2,1)} %param.23) | copy-start | bytes 12292
